TPU v7x, 32 devices: a whole 2x2x4 slice. The times are simulated.
32 devices in a mesh: grp: 2 (over x), tp: 16 (over z, y, core).
Axes of the slice: x: 2, y: 2, z: 4, core: 2. Of those that a mesh axis runs over, the one named last changes fastest.
Arguments:
- tokens: bfloat16 [96, 4096], P('grp', 'tp'), parts along dimension 0, may hold values from -6 to 6
- states: float32 [2, 96, 32, 128, 128], P(None, 'grp', 'tp'), parts along dimension 1, may hold values from -10 to 10
- norm_gain: float32 [2, 4096], replicated, may hold values from 0.1 to 1.9
- query_weight: bfloat16 [2, 4096, 4096], P(None, None, 'tp'), may hold values from -0.09375 to 0.09375
- forget_weight: bfloat16 [2, 4096, 4096], P(None, None, 'tp'), may hold values from -0.09375 to 0.09375
- value_weight: bfloat16 [2, 4096, 4096], P(None, None, 'tp'), may hold values from -0.09375 to 0.09375
- gate_weight: bfloat16 [2, 4096, 4096], P(None, None, 'tp'), may hold values from -0.09375 to 0.09375
- output_weight: bfloat16 [2, 4096, 4096], P(None, 'tp'), may hold values from -0.125 to 0.125
- output_gain: float32 [2, 4096], P(None, 'tp'), may hold values from 0.1 to 1.9
- bound_logits: float32 [4096], P('tp'), may hold values from -6 to 6
Outputs:
- mixed: bfloat16 [96, 4096], P('grp', 'tp'), parts along dimension 0
- new_states: float32 [2, 96, 32, 128, 128], P(None, 'grp', 'tp'), parts along dimension 1
There are 2 independent parts, one for each index of `grp`. A program takes and returns all parts, laid end to end along the dimension named above; an argument that names none is the same for every part. Nothing has to cross between parts.
All inputs are finite; a program needn't handle non-finite values.
Results may differ from a plain program's by a relative error of at most 0.017.
Values may be sent and summed in bfloat16 or wider, within the bound.
A program may use at most 128 MiB of HBM per device.

v0:
```python
import jax
import jax.numpy as jnp
from jax import lax
from jax.sharding import PartitionSpec as P

epsilon = 1e-06


def mixer_step(
    gathered,
    state_in,
    gain_in,
    query_mat,
    forget_mat,
    value_mat,
    gate_mat,
    out_mat,
    gain_out,
    lower_bound,
):
    stream32 = gathered.astype(jnp.float32)
    factor = lax.rsqrt(jnp.mean(stream32 * stream32, axis=-1, keepdims=True) + epsilon)
    normed = (stream32 * factor * gain_in).astype(jnp.bfloat16)
    query_proj = jnp.dot(normed, query_mat, preferred_element_type=jnp.float32).astype(jnp.bfloat16)
    forget_pre = jnp.dot(normed, forget_mat, preferred_element_type=jnp.float32).astype(
        jnp.bfloat16
    )
    value_proj = jnp.dot(normed, value_mat, preferred_element_type=jnp.float32).astype(jnp.bfloat16)
    gate_proj = jnp.dot(normed, gate_mat, preferred_element_type=jnp.float32).astype(jnp.bfloat16)
    forget = lower_bound + (1.0 - lower_bound) * jax.nn.sigmoid(forget_pre.astype(jnp.float32))
    rows = gathered.shape[0]
    heads_local = state_in.shape[1]
    head_size = state_in.shape[2]
    forget_heads = forget.reshape(rows, heads_local, head_size)
    value_heads = value_proj.astype(jnp.float32).reshape(rows, heads_local, head_size)
    query_heads = query_proj.astype(jnp.float32).reshape(
        rows, heads_local, head_size
    ) * head_size ** (-0.5)
    updated = (
        forget_heads[..., None] * state_in
        + (1.0 - forget_heads)[..., None] * value_heads[:, :, None, :]
    )
    readout = jnp.einsum(
        "bhk,bhkv->bhv", query_heads, updated, precision=lax.Precision.HIGHEST
    ).reshape(rows, heads_local * head_size)
    energy = jnp.sum(readout * readout, axis=-1)
    gated_rows = (readout * gain_out * jax.nn.silu(gate_proj.astype(jnp.float32))).astype(
        jnp.bfloat16
    )
    partial_value = jnp.dot(gated_rows, out_mat, preferred_element_type=jnp.float32)
    return (updated, partial_value, energy)


def body(
    tokens,
    states,
    norm_gain,
    query_weight,
    forget_weight,
    value_weight,
    gate_weight,
    output_weight,
    output_gain,
    bound_logits,
):
    devices = lax.axis_size("tp")
    columns = tokens.shape[1]
    model_width = columns * devices
    rows = tokens.shape[0]
    gathered = lax.all_gather(tokens, "tp", axis=1, tiled=True)
    state_first, partial_value, energy = mixer_step(
        gathered,
        states[0],
        norm_gain[0],
        query_weight[0],
        forget_weight[0],
        value_weight[0],
        gate_weight[0],
        output_weight[0],
        output_gain[0],
        0.0,
    )
    owned_sums, energies = (
        lax.psum_scatter(partial_value, "tp", scatter_dimension=1, tiled=True),
        lax.psum_scatter(
            jnp.broadcast_to(energy[:, None], (rows, devices)),
            "tp",
            scatter_dimension=1,
            tiled=True,
        ),
    )
    rescale = lax.rsqrt(energies / model_width + epsilon)
    middle = (tokens.astype(jnp.float32) + owned_sums * rescale).astype(jnp.bfloat16)
    middle_full = lax.all_gather(middle, "tp", axis=1, tiled=True)
    state_second, partial_value, energy = mixer_step(
        middle_full,
        states[1],
        norm_gain[1],
        query_weight[1],
        forget_weight[1],
        value_weight[1],
        gate_weight[1],
        output_weight[1],
        output_gain[1],
        jax.nn.sigmoid(bound_logits),
    )
    owned_sums, energies = (
        lax.psum_scatter(partial_value, "tp", scatter_dimension=1, tiled=True),
        lax.psum_scatter(
            jnp.broadcast_to(energy[:, None], (rows, devices)),
            "tp",
            scatter_dimension=1,
            tiled=True,
        ),
    )
    rescale = lax.rsqrt(energies / model_width + epsilon)
    mixed = (middle.astype(jnp.float32) + owned_sums * rescale).astype(jnp.bfloat16)
    return (mixed, jnp.stack([state_first, state_second]))


def solution(mesh):
    placed = (
        P("grp", "tp"),
        P(None, "grp", "tp", None, None),
        P(),
        P(None, None, "tp"),
        P(None, None, "tp"),
        P(None, None, "tp"),
        P(None, None, "tp"),
        P(None, "tp", None),
        P(None, "tp"),
        P("tp"),
    )
    return jax.shard_map(
        body,
        mesh=mesh,
        in_specs=placed,
        out_specs=(P("grp", "tp"), P(None, "grp", "tp", None, None)),
        check_vma=False,
    )
```

profile of v0, /device:TPU:0, one launch (start us, length us, event | category | flops | bytes accessed | tf_op | source)
XLA Modules:
  0.0 242.1 jit_solution(17751710673130286631)
XLA Ops:
  7.2 0.0 reduce-scatter.3.cloned.1.call-start
  7.2 0.8 fusion.169
  8.0 0.9 fusion.168
  8.8 24.4 %all_gather.6 = bf16[48,4096]{1,0:T(8,128)(2,1)S(1)} all-gather(bf16[48,256]{1,0:T(8,128)(2,1)} %param.10), channel_id=1, replica_groups=mesh['grp'=2,'tp'=16] {'tp'}, dimensions={1}, use_global_device_ids=true | all-gather | bytes 417792 | tf_op jit(solution)/shard_map/all_gather | solution.py:70
  33.3 0.2 fusion.130
  33.5 2.1 fusion.70
  35.7 2.1 fusion.76
  37.8 2.1 fusion.52
  40.0 9.5 %fusion.4 = f32[48,2,1,128]{3,2,1,0:T(1,128)S(1)} fusion(f32[48,2,128,1]{2,3,1,0:T(1,128)S(1)} %bitcast.151, f32[2,48,2,128,128]{4,3,2,1,0:T(8,128)} %param.11, f32[48,2,128]{2,1,0:T(2,128)S(1)} %reshape.60, f32[48,2,128]{2,1,0:T(2,128)S(1)} %broadcast_subtract_fusion.1, f32[48,2,128]{2,1,0:T(2,128)S(1)} %mul.223), kind=kOutput, calls=%fused_computation.6 | convolution fusion | flops 23592960 | bytes 6537216 | tf_op jit(solution)/shard_map/bhk,bhkv->bhv/dot_general | solution.py:43
  49.4 0.0 copy-start.3
  49.4 0.0 copy-start.1
  49.5 0.0 copy-start
  49.5 4.5 %fusion.26 = f32[48,4096]{1,0:T(8,128)} fusion(bf16[2,256,4096]{2,1,0:T(8,128)(2,1)} %param.17, f32[6,8,2,128]{3,2,1,0:T(2,128)S(1)} %bitcast.139, bf16[2,4096,256]{2,1,0:T(8,128)(2,1)} %param.16, f32[256]{0:T(256)S(1)} %bitcast.154, bf16[48,4096]{1,0:T(8,128)(2,1)S(1)} %all_gather.6, f32[4096]{0:T(1024)S(1)} %bitcast.150, f32[48]{0:T(128)S(1)} %add_rsqrt_fusion.1), kind=kOutput, calls=%fused_computation.29 | convolution fusion | flops 202223616 | bytes 5440704 | tf_op jit(solution)/shard_map/dot_general | solution.py:50
  53.9 0.0 reduce-scatter.3.cloned.1.call-update
  54.0 0.0 reduce-scatter.5.cloned.1.call-start
  54.0 0.0 copy-done.3
  54.0 0.6 dynamic-slice
  54.6 0.4 multiply_reduce_fusion.1
  55.1 30.5 %all-reduce = f32[48,16]{0,1:T(8,128)S(1)} all-reduce(f32[48,16]{0,1:T(8,128)S(1)} %broadcast_in_dim.4), channel_id=3, replica_groups=mesh['grp'=2,'tp'=16] {'tp'}, use_global_device_ids=true, to_apply=%region_3.4.clone | all-reduce | flops 768 | bytes 6144
  85.6 0.7 rsqrt_bitcast_fusion.1
  86.2 0.0 copy-done.1
  86.3 21.9 %reduce-scatter.3.cloned.1.call-done = f32[48,256]{1,0:T(8,128)} async-done(((f32[48,4096]{1,0:T(8,128)}), f32[48,256]{1,0:T(8,128)}) %reduce-scatter.3.cloned.1.call-update) | async-done | bytes 49168 | tf_op jit(solution)/shard_map/reduce_scatter | solution.py:84
  108.2 0.0 copy-done
  108.2 0.0 copy-start.2
  108.2 1.0 add_convert_fusion.1
  109.2 20.6 %all_gather.7 = bf16[48,4096]{1,0:T(8,128)(2,1)S(1)} all-gather(bf16[48,256]{1,0:T(8,128)(2,1)S(1)} %add_convert_fusion.1), channel_id=1, replica_groups=mesh['grp'=2,'tp'=16] {'tp'}, dimensions={1}, use_global_device_ids=true | all-gather | bytes 417792 | tf_op jit(solution)/shard_map/all_gather | solution.py:94
  129.8 0.2 fusion.133
  130.0 2.1 fusion.121
  132.1 2.1 fusion.91
  134.2 0.0 copy-done.2
  134.3 0.5 fusion.115
  134.9 9.5 %fusion.1 = f32[48,2,1,128]{3,2,1,0:T(1,128)S(1)} fusion(f32[48,2,128,1]{2,3,1,0:T(1,128)S(1)} %bitcast.152, f32[2,48,2,128,128]{4,3,2,1,0:T(8,128)} %param.11, f32[48,2,128]{2,1,0:T(2,128)S(1)} %reshape.61, f32[48,2,128]{2,1,0:T(2,128)S(1)} %broadcast_subtract_fusion, f32[48,2,128]{2,1,0:T(2,128)S(1)} %mul.250), kind=kOutput, calls=%fused_computation.3 | convolution fusion | flops 23592960 | bytes 6537216 | tf_op jit(solution)/shard_map/bhk,bhkv->bhv/dot_general | solution.py:43
  144.4 0.4 multiply_reduce_fusion
  144.8 30.3 %all-reduce.1 = f32[48,16]{0,1:T(8,128)S(1)} all-reduce(f32[48,16]{0,1:T(8,128)S(1)} %broadcast_in_dim.5), channel_id=5, replica_groups=mesh['grp'=2,'tp'=16] {'tp'}, use_global_device_ids=true, to_apply=%region_7.8.clone | all-reduce | flops 768 | bytes 6144
  175.2 4.5 %fusion.16 = f32[48,4096]{1,0:T(8,128)} fusion(bf16[2,256,4096]{2,1,0:T(8,128)(2,1)} %param.17, f32[6,8,2,128]{3,2,1,0:T(2,128)S(1)} %bitcast.142, bf16[2,4096,256]{2,1,0:T(8,128)(2,1)} %param.16, f32[256]{0:T(256)S(1)} %bitcast.153, bf16[48,4096]{1,0:T(8,128)(2,1)S(1)} %all_gather.7, f32[4096]{0:T(1024)S(1)} %bitcast.146, f32[48]{0:T(128)S(1)} %add_rsqrt_fusion), kind=kOutput, calls=%fused_computation.19 | convolution fusion | flops 202223616 | bytes 5440704 | tf_op jit(solution)/shard_map/dot_general | solution.py:50
  179.6 0.0 reduce-scatter.5.cloned.1.call-update
  179.7 0.7 rsqrt_bitcast_fusion
  180.3 9.8 %multiply_add_fusion.1 = (f32[1,48,2,128,128]{4,3,2,1,0:T(8,128)S(1)}, f32[1,48,2,128,128]{4,3,2,1,0:T(8,128)}) fusion(f32[2,48,2,128,128]{4,3,2,1,0:T(8,128)} %param.11, f32[48,2,128]{2,1,0:T(2,128)S(1)} %reshape.60, f32[48,2,128]{2,1,0:T(2,128)S(1)} %broadcast_subtract_fusion.1, f32[48,2,128]{2,1,0:T(2,128)S(1)} %mul.223, f32[48,2,128]{2,1,0:T(2,128)S(1)} %reshape.61, ...), kind=kLoop, calls=%fused_computation.8 | loop fusion | flops 9437184 | bytes 25460736 | tf_op jit(solution)/shard_map/add | solution.py:40
  190.1 9.3 %pad_maximum_fusion = f32[2,48,2,128,128]{4,3,2,1,0:T(8,128)} fusion(f32[1,48,2,128,128]{4,3,2,1,0:T(8,128)} %get-tuple-element.5, f32[1,48,2,128,128]{4,3,2,1,0:T(8,128)S(1)} %get-tuple-element.4), kind=kLoop, calls=%fused_computation | loop fusion | flops 3145728 | bytes 25165824 | tf_op jit(solution)/shard_map/stack | solution.py:118
  199.4 34.4 %reduce-scatter.5.cloned.1.call-done = f32[48,256]{1,0:T(8,128)} async-done(((f32[48,4096]{1,0:T(8,128)}), f32[48,256]{1,0:T(8,128)}) %reduce-scatter.5.cloned.1.call-update) | async-done | bytes 49168 | tf_op jit(solution)/shard_map/reduce_scatter | solution.py:108
  233.8 1.5 add_convert_fusion
  (13 shorter events, 0.2 us)
Async XLA Ops:
  7.2 101.0 %reduce-scatter.3.cloned.1.call-start = ((), (), s32[]{:S(2)}) async-start(), calls=%async_computation.2 | async-start | bytes 835584 | tf_op jit(solution)/shard_map/reduce_scatter | solution.py:84
  49.4 4.6 %copy-start.3 = (u32[32]{0:T(128)S(1)}, u32[32]{0:T(128)}, u32[]{:S(2)}) copy-start(u32[32]{0:T(128)} %constant.22) | copy-start | bytes 388
  49.4 36.8 %copy-start.1 = (f32[256]{0:T(256)S(1)}, f32[256]{0:T(256)}, u32[]{:S(2)}) copy-start(f32[256]{0:T(256)} %param.19) | copy-start | bytes 3076
  49.5 58.7 %copy-start = (bf16[48,256]{1,0:T(8,128)(2,1)S(1)}, bf16[48,256]{1,0:T(8,128)(2,1)}, u32[]{:S(2)}) copy-start(bf16[48,256]{1,0:T(8,128)(2,1)} %param.10) | copy-start | bytes 73732
  54.0 179.8 %reduce-scatter.5.cloned.1.call-start = ((), (), s32[]{:S(2)}) async-start(), calls=%async_computation.3 | async-start | bytes 835584 | tf_op jit(solution)/shard_map/reduce_scatter | solution.py:108
  108.2 26.1 %copy-start.2 = (bf16[2,4096,256]{2,1,0:T(8,128)(2,1)S(1)}, bf16[2,4096,256]{2,1,0:T(8,128)(2,1)}, u32[]{:S(2)}) copy-start(bf16[2,4096,256]{2,1,0:T(8,128)(2,1)} %param.14) | copy-start | bytes 12582916
Sparse Core Ops, SparseCore 0:
  54.1 54.0 reduce-scatter.2
  179.8 53.9 reduce-scatter.4
where the time goes:
time: 243 us; the launch traced here: 242 us
  blocking collectives  106 us (44%)
  waiting for transfers between devices  56.3 us (23%)
  matrix products  38.9 us (16%)
  other arithmetic  24.2 us (10%)
  between operations  14.2 us (6%)
    unnamed x2, blocking collectives  60.8 us
    reduce_scatter x2, waiting for transfers between devices, body(): lax.psum_scatter(partial_value, 'tp', scatter_dimension=1, tiled=True)  56.3 us
    all_gather x1, blocking collectives, body(): gathered = lax.all_gather(tokens, 'tp', axis=1, tiled=True)  24.4 us
    all_gather x1, blocking collectives, body(): middle_full = lax.all_gather(middle, 'tp', axis=1, tiled=True)  20.6 us
    dot_general x2, matrix products, mixer_step(): jnp.einsum('bhk,bhkv->bhv', query_heads, updated, precision=lax.Precision...  18.9 us
    add x1, other arithmetic, mixer_step(): forget_heads[..., None] * state_in  9.79 us
    another operation x1, other arithmetic, body(): return (mixed, jnp.stack([state_first, state_second]))  9.28 us
    dot_general x2, matrix products, mixer_step(): jnp.dot(gated_rows, out_mat, preferred_element_type=jnp.float32)  8.93 us
  transfers between devices with their start and end apart: 2, of which 2 were waited for; matrix products, arithmetic and copies ran while one was open for 9% of the time, Pallas kernels for 0%

commit v1 on v0

v1 whole, which is shorter than its diff:
```python
import functools

import jax
import jax.numpy as jnp
from jax import lax
from jax.experimental import pallas as pl
from jax.experimental.pallas import tpu as pltpu
from jax.sharding import PartitionSpec as P

epsilon = 1e-06


def kernel(
    n,
    tok,
    states,
    gain,
    wq,
    wf,
    wv,
    wg,
    wo,
    ogain,
    blog,
    mixed,
    new,
    w_s,
    wo_s,
    gain_s,
    ogain_s,
    blog_s,
    xg,
    acc,
    ss,
    tf,
    tq,
    v_s,
    ro_s,
    g_s,
    sb,
    ra,
    pb,
    rb,
    es,
    er,
    ep,
    eb,
    sm_sem,
    w_sem,
    gs,
    gr,
    fs,
    fr,
    asend,
    arecv,
    bsend,
    brecv,
    essend,
    esrecv,
    ebsend,
    ebrecv,
):
    rows, cols = tok.shape
    width = cols * n
    heads = states.shape[2]
    size = states.shape[3]
    groups = rows // 8
    half = n // 2
    me = lax.axis_index("tp")
    sib = me + 1 - 2 * lax.rem(me, 2)

    def peer(s):
        return lax.rem(me + 2 * s, n)

    def origin(s):
        return lax.rem(me - 2 * s + n, n)

    def sib_origin(s):
        return lax.rem(sib - 2 * s + n, n)

    def span(d):
        return pl.ds(pl.multiple_of(d * cols, cols), cols)

    def remote(src, dst, send, recv, d):
        return pltpu.make_async_remote_copy(
            src_ref=src,
            dst_ref=dst,
            send_sem=send,
            recv_sem=recv,
            device_id={"tp": d},
            device_id_type=pl.DeviceIdType.MESH,
        )

    barrier = pltpu.get_barrier_semaphore()

    def greet(d):
        pl.semaphore_signal(
            barrier, inc=1, device_id={"tp": d}, device_id_type=pl.DeviceIdType.MESH
        )

    greet(sib)

    @pl.loop(1, half)
    def _(s):
        greet(peer(s))

    tok_copy = pltpu.make_async_copy(tok, xg.at[0, me], sm_sem.at[0])
    tok_copy.start()
    gain_copy = pltpu.make_async_copy(gain, gain_s, sm_sem.at[1])
    gain_copy.start()
    og_copy = pltpu.make_async_copy(ogain, ogain_s, sm_sem.at[2])
    og_copy.start()
    bl_copy = pltpu.make_async_copy(blog, blog_s, sm_sem.at[3])
    bl_copy.start()

    def weight_copies(l):
        return [
            pltpu.make_async_copy(w.at[l], w_s.at[l, i], w_sem.at[l, i])
            for i, w in enumerate((wq, wf, wv, wg))
        ]

    def later_copies(l):
        return [
            pltpu.make_async_copy(states.at[l], new.at[l], w_sem.at[l, 4]),
            pltpu.make_async_copy(wo.at[l], wo_s.at[l], w_sem.at[l, 5]),
        ]

    for c in weight_copies(0):
        c.start()
    for c in later_copies(0):
        c.start()
    for c in weight_copies(1):
        c.start()
    for c in later_copies(1):
        c.start()
    pl.semaphore_wait(barrier, half)
    tok_copy.wait()

    def gather_copy(l, s):
        return remote(xg.at[l, me], xg.at[l, me], gs.at[l, s], gr.at[l, s], peer(s))

    def forward_copy(l, s):
        o = origin(s)
        return remote(xg.at[l, o], xg.at[l, o], fs.at[l, s], fr.at[l, s], sib)

    def a_copy(l, s):
        return remote(sb.at[l, s], ra.at[l, s], asend.at[l, s], arecv.at[l, s], sib)

    def b_copy(l, s):
        return remote(pb.at[l, s], rb.at[l, s], bsend.at[l, s], brecv.at[l, s], peer(s))

    def es_copy(l):
        return remote(es.at[l], er.at[l], essend.at[l], esrecv.at[l], sib)

    def eb_copy(l, s):
        return remote(ep.at[l], eb.at[l, s], ebsend.at[l, s], ebrecv.at[l, s], peer(s))

    for l in range(2):
        forward_copy(l, 0).start()

        @pl.loop(1, half)
        def _(s):
            gather_copy(l, s).start()

        acc[...] = jnp.zeros_like(acc)
        ss[...] = jnp.zeros_like(ss)

        def chunk(o):
            x = xg[l, o].astype(jnp.float32)
            square = x * x
            total = square[:, :128]
            for c in range(128, cols, 128):
                total = total + square[:, c : c + 128]
            ss[...] += total
            scaled = (x * gain_s[l : l + 1, span(o)]).astype(jnp.bfloat16)
            for i in range(4):
                acc[i] += jnp.dot(
                    scaled, w_s[l, i, span(o), :], preferred_element_type=jnp.float32
                )

        if l == 0:
            gain_copy.wait()
        for c in weight_copies(l):
            c.wait()
        chunk(me)

        @pl.loop(1, half)
        def _(s):
            gather_copy(l, s).wait_recv()
            forward_copy(l, s).start()
            chunk(origin(s))
            forward_copy(l, s - 1).wait_recv()
            chunk(sib_origin(s - 1))

        forward_copy(l, half - 1).wait_recv()
        chunk(sib_origin(half - 1))

        factor = lax.rsqrt(jnp.sum(ss[...], axis=-1, keepdims=True) / width + epsilon)

        def projected(i):
            return (acc[i] * factor).astype(jnp.bfloat16).astype(jnp.float32)

        if l == 0:
            og_copy.wait()
            bl_copy.wait()
        query = projected(0) * size**-0.5
        forget = jax.nn.sigmoid(projected(1))
        if l == 1:
            lower = jax.nn.sigmoid(blog_s[...])
            forget = lower + (1.0 - lower) * forget
        v_s[...] = projected(2)
        pad = jnp.zeros((size - rows, size), jnp.float32)
        for h in range(heads):
            for source, dest in ((forget, tf), (query, tq)):
                part = source[:, h * size : (h + 1) * size]
                flipped = jnp.concatenate([part, pad], axis=0).T
                for b in range(groups):
                    shift = (size - 8 * b) % size
                    dest[b, h] = pltpu.roll(flipped, shift, 1) if shift else flipped
        state_copy, wo_copy = later_copies(l)
        state_copy.wait()

        @pl.loop(0, groups)
        def _(b):
            base = pl.multiple_of(b * 8, 8)
            for h in range(heads):
                lanes = slice(h * size, (h + 1) * size)
                values = v_s[pl.ds(base, 8), lanes]
                lines = []
                for j in range(8):
                    value = values[j : j + 1, :]
                    keep = tf[b, h, :, j : j + 1]
                    ask = tq[b, h, :, j : j + 1]
                    updated = keep * (new[l, base + j, h] - value) + value
                    new[l, base + j, h] = updated
                    lines.append(jnp.sum(ask * updated, axis=0, keepdims=True))
                ro_s[pl.ds(base, 8), lanes] = jnp.concatenate(lines, axis=0)

        readout = ro_s[...]
        energy = jnp.sum(readout * readout, axis=-1, keepdims=True)
        lane = lax.broadcasted_iota(jnp.int32, (8, 128), 1)
        tile = jnp.zeros((8, 128), jnp.float32)
        for b in range(groups):
            tile = jnp.where(lane == b, energy[8 * b : 8 * b + 8], tile)
        es[l] = tile
        g_s[...] = (readout * ogain_s[l : l + 1, :] * jax.nn.silu(projected(3))).astype(
            jnp.bfloat16
        )
        es_copy(l).start()
        wo_copy.wait()

        def product(d):
            return jnp.dot(
                g_s[...], wo_s[l, :, span(d)], preferred_element_type=jnp.float32
            )

        @pl.loop(0, half)
        def _(t):
            s = lax.rem(t + 1, half)
            sb[l, s] = product(lax.rem(sib + 2 * s, n)).astype(jnp.bfloat16)
            a_copy(l, s).start()

        es_copy(l).wait_recv()
        ep[l] = es[l] + er[l]

        @pl.loop(1, half)
        def _(s):
            eb_copy(l, s).start()
            mine = product(peer(s))
            a_copy(l, s).wait_recv()
            pb[l, s] = (mine + ra[l, s].astype(jnp.float32)).astype(jnp.bfloat16)
            b_copy(l, s).start()

        mine = product(me)
        a_copy(l, 0).wait_recv()
        mine = mine + ra[l, 0].astype(jnp.float32)

        def collect(s, carry):
            total, powers = carry
            eb_copy(l, s).wait_recv()
            b_copy(l, s).wait_recv()
            return total + rb[l, s].astype(jnp.float32), powers + eb[l, s]

        total, powers = lax.fori_loop(1, half, collect, (mine, ep[l]))
        column = jnp.concatenate([powers[:, b : b + 1] for b in range(groups)], axis=0)
        rescale = lax.rsqrt(column / width + epsilon)
        stream = (xg[l, me].astype(jnp.float32) + total * rescale).astype(jnp.bfloat16)
        if l == 0:
            xg[1, me] = stream
        else:
            mixed[...] = stream

    for l in range(2):
        forward_copy(l, 0).wait_send()
        a_copy(l, 0).wait_send()
        es_copy(l).wait_send()

        @pl.loop(1, half)
        def _(s):
            gather_copy(l, s).wait_send()
            forward_copy(l, s).wait_send()
            a_copy(l, s).wait_send()
            b_copy(l, s).wait_send()
            eb_copy(l, s).wait_send()


def body(
    n,
    tokens,
    states,
    norm_gain,
    query_weight,
    forget_weight,
    value_weight,
    gate_weight,
    output_weight,
    output_gain,
    bound_logits,
):
    rows, cols = tokens.shape
    width = cols * n
    heads, size = states.shape[2:4]
    groups = rows // 8
    half = n // 2
    f32, b16 = jnp.float32, jnp.bfloat16
    dma = pltpu.SemaphoreType.DMA
    anywhere = pl.BlockSpec(memory_space=pl.ANY)
    in_vmem = pl.BlockSpec(memory_space=pltpu.VMEM)
    mixed, new = pl.pallas_call(
        functools.partial(kernel, n),
        out_shape=(
            jax.ShapeDtypeStruct(tokens.shape, b16),
            pltpu.VMEM(states.shape, f32),
        ),
        in_specs=[anywhere] * 10,
        out_specs=(in_vmem, in_vmem),
        scratch_shapes=[
            pltpu.VMEM((2, 4, width, cols), b16),
            pltpu.VMEM((2, cols, width), b16),
            pltpu.VMEM((2, width), f32),
            pltpu.VMEM((2, cols), f32),
            pltpu.VMEM((1, cols), f32),
            pltpu.VMEM((2, n, rows, cols), b16),
            pltpu.VMEM((4, rows, cols), f32),
            pltpu.VMEM((rows, 128), f32),
            pltpu.VMEM((groups, heads, size, size), f32),
            pltpu.VMEM((groups, heads, size, size), f32),
            pltpu.VMEM((rows, cols), f32),
            pltpu.VMEM((rows, cols), f32),
            pltpu.VMEM((rows, cols), b16),
            pltpu.VMEM((2, half, rows, cols), b16),
            pltpu.VMEM((2, half, rows, cols), b16),
            pltpu.VMEM((2, half, rows, cols), b16),
            pltpu.VMEM((2, half, rows, cols), b16),
            pltpu.VMEM((2, 8, 128), f32),
            pltpu.VMEM((2, 8, 128), f32),
            pltpu.VMEM((2, 8, 128), f32),
            pltpu.VMEM((2, half, 8, 128), f32),
            dma((4,)),
            dma((2, 6)),
            dma((2, half)),
            dma((2, half)),
            dma((2, half)),
            dma((2, half)),
            dma((2, half)),
            dma((2, half)),
            dma((2, half)),
            dma((2, half)),
            dma((2,)),
            dma((2,)),
            dma((2, half)),
            dma((2, half)),
        ],
        compiler_params=pltpu.CompilerParams(
            collective_id=0, has_side_effects=True, vmem_limit_bytes=46000 * 1024
        ),
    )(
        tokens,
        states,
        norm_gain,
        query_weight,
        forget_weight,
        value_weight,
        gate_weight,
        output_weight,
        output_gain,
        bound_logits.reshape(1, cols),
    )
    return mixed, new


def solution(mesh):
    placed = (
        P("grp", "tp"),
        P(None, "grp", "tp", None, None),
        P(),
        P(None, None, "tp"),
        P(None, None, "tp"),
        P(None, None, "tp"),
        P(None, None, "tp"),
        P(None, "tp", None),
        P(None, "tp"),
        P("tp"),
    )
    return jax.shard_map(
        functools.partial(body, mesh.shape["tp"]),
        mesh=mesh,
        in_specs=placed,
        out_specs=(P("grp", "tp"), P(None, "grp", "tp", None, None)),
        check_vma=False,
    )
```

time: 243 us -> 63.1 us (0.26)
  blocking collectives: 106 us -> 0 us
  Pallas kernels: 0 us -> 56.9 us
  waiting for transfers between devices: 56.3 us -> 0 us
  matrix products: 38.9 us -> 0 us
  other arithmetic: 24.2 us -> 0 us
  between operations: 14.2 us -> 0.65 us
  local copies, waits for them, and re-layouts: 2.4 us -> 5.39 us
    unnamed x2 -> x0, blocking collectives: 60.8 us -> none
    pallas_call x0 -> x1, Pallas kernels: none -> 56.9 us  [body(): pl.pallas_call(functools.partial(kernel, n), out_shape=(jax.ShapeDtypeStr...]
    reduce_scatter x2 -> x0, waiting for transfers between devices: 56.3 us -> none  [body(): lax.psum_scatter(partial_value, 'tp', scatter_dimension=1, tiled=True)]
    all_gather x2 -> x0, blocking collectives: 45 us -> none  [the longest x1 24.4 us: body(): gathered = lax.all_gather(tokens, 'tp', axis=1, tiled=True)]
    dot_general x10 -> x0, matrix products: 38.9 us -> none  [the longest x2 18.9 us: mixer_step(): jnp.einsum('bhk,bhkv->bhv', query_heads, updated, precision=lax.Precision...]
    add x1 -> x0, other arithmetic: 9.79 us -> none  [mixer_step(): forget_heads[..., None] * state_in]
    another operation x1 -> x0, other arithmetic: 9.28 us -> none  [body(): return (mixed, jnp.stack([state_first, state_second]))]
    unnamed x9 -> x4, local copies, waits for them, and re-layouts: 0.61 us -> 5.39 us
  transfers between devices with their start and end apart: 2 -> 0, of which waited for: 2 -> 0; matrix products, arithmetic and copies ran while one was open for 9% -> 0% of each run, Pallas kernels for 0% -> 0%
where the time goes in v1:
time: 63.1 us; the launch traced here: 63 us
  Pallas kernels  56.9 us (90%)
  local copies, waits for them, and re-layouts  5.39 us (9%)
  between operations  0.65 us (1%)
    pallas_call x1, Pallas kernels, body(): pl.pallas_call(functools.partial(kernel, n), out_shape=(jax.ShapeDtypeStr...  56.9 us
    unnamed x4, local copies, waits for them, and re-layouts  5.39 us

profile of v1, /device:TPU:0, one launch (start us, length us, event | category | flops | bytes accessed | tf_op | source)
XLA Modules:
  0.0 63.0 jit_solution(7958243251854046951)
XLA Ops:
  0.6 56.9 %shard_map.113 = (bf16[48,256]{1,0:T(8,128)(2,1)}, f32[2,48,2,128,128]{4,3,2,1,0:T(8,128)S(1)}) custom-call(bf16[48,256]{1,0:T(8,128)(2,1)} %tok.1, f32[2,48,2,128,128]{4,3,2,1,0:T(8,128)} %states.1, f32[2,4096]{1,0:T(2,128)} %gain.1, bf16[2,4096,256]{2,1,0:T(8,128)(2,1)} %wq.1, bf16[2,4096,256]{2,1,0:T(8,128)(2,1)} %wf.1, bf16[2,4096,256]{2,1,0:T(8,128)(2,1)} %wv.1, ...), custom_call_target="tpu_custom_call" | custom-call | tf_op jit(solution)/shard_map/pallas_call | solution.py:329
  57.6 0.0 copy-start
  57.6 4.8 %copy.14 = f32[2,48,2,128,128]{4,3,2,1,0:T(8,128)} copy(f32[2,48,2,128,128]{4,3,2,1,0:T(8,128)S(1)} %get-tuple-element.3) | data formatting | bytes 25165824
  62.4 0.0 copy-done
  62.4 0.6 copy.15
Async XLA Ops:
  57.6 4.8 %copy-start = (bf16[48,256]{1,0:T(8,128)(2,1)S(1)}, bf16[48,256]{1,0:T(8,128)(2,1)}, u32[]{:S(2)}) copy-start(bf16[48,256]{1,0:T(8,128)(2,1)} %get-tuple-element.6) | copy-start | bytes 73732

commit v2 on v1

--- a/solution.py
+++ b/solution.py
@@ -127,12 +127,6 @@
 
     for c in weight_copies(0):
         c.start()
-    for c in later_copies(0):
-        c.start()
-    for c in weight_copies(1):
-        c.start()
-    for c in later_copies(1):
-        c.start()
     pl.semaphore_wait(barrier, half)
     tok_copy.wait()
 
@@ -182,18 +176,23 @@
             gain_copy.wait()
         for c in weight_copies(l):
             c.wait()
+        if l == 0:
+            for c in later_copies(0):
+                c.start()
         chunk(me)
+        forward_copy(l, 0).wait_recv()
+        chunk(sib_origin(0))
 
         @pl.loop(1, half)
         def _(s):
             gather_copy(l, s).wait_recv()
             forward_copy(l, s).start()
             chunk(origin(s))
-            forward_copy(l, s - 1).wait_recv()
-            chunk(sib_origin(s - 1))
-
-        forward_copy(l, half - 1).wait_recv()
-        chunk(sib_origin(half - 1))
+
+        @pl.loop(1, half)
+        def _(s):
+            forward_copy(l, s).wait_recv()
+            chunk(sib_origin(s))
 
         factor = lax.rsqrt(jnp.sum(ss[...], axis=-1, keepdims=True) / width + epsilon)
 
@@ -208,15 +207,21 @@
         if l == 1:
             lower = jax.nn.sigmoid(blog_s[...])
             forget = lower + (1.0 - lower) * forget
-        v_s[...] = projected(2)
+        value = projected(2)
+        v_s[...] = value
+        kept = query * forget
+        fresh = query - kept
         pad = jnp.zeros((size - rows, size), jnp.float32)
-        for h in range(heads):
-            for source, dest in ((forget, tf), (query, tq)):
+
+        def flip(source, dest):
+            for h in range(heads):
                 part = source[:, h * size : (h + 1) * size]
                 flipped = jnp.concatenate([part, pad], axis=0).T
                 for b in range(groups):
                     shift = (size - 8 * b) % size
                     dest[b, h] = pltpu.roll(flipped, shift, 1) if shift else flipped
+
+        flip(kept, tq)
         state_copy, wo_copy = later_copies(l)
         state_copy.wait()
 
@@ -225,16 +230,18 @@
             base = pl.multiple_of(b * 8, 8)
             for h in range(heads):
                 lanes = slice(h * size, (h + 1) * size)
-                values = v_s[pl.ds(base, 8), lanes]
                 lines = []
                 for j in range(8):
-                    value = values[j : j + 1, :]
-                    keep = tf[b, h, :, j : j + 1]
                     ask = tq[b, h, :, j : j + 1]
-                    updated = keep * (new[l, base + j, h] - value) + value
-                    new[l, base + j, h] = updated
-                    lines.append(jnp.sum(ask * updated, axis=0, keepdims=True))
+                    lines.append(
+                        jnp.sum(ask * new[l, base + j, h], axis=0, keepdims=True)
+                    )
                 ro_s[pl.ds(base, 8), lanes] = jnp.concatenate(lines, axis=0)
+
+        for h in range(heads):
+            lanes = slice(h * size, (h + 1) * size)
+            share = jnp.sum(fresh[:, lanes], axis=-1, keepdims=True)
+            ro_s[:, lanes] += share * value[:, lanes]
 
         readout = ro_s[...]
         energy = jnp.sum(readout * readout, axis=-1, keepdims=True)
@@ -248,6 +255,9 @@
         )
         es_copy(l).start()
         wo_copy.wait()
+        if l == 0:
+            for c in weight_copies(1) + later_copies(1):
+                c.start()
 
         def product(d):
             return jnp.dot(
@@ -274,6 +284,18 @@
         mine = product(me)
         a_copy(l, 0).wait_recv()
         mine = mine + ra[l, 0].astype(jnp.float32)
+
+        flip(forget, tf)
+
+        @pl.loop(0, groups)
+        def _(b):
+            base = pl.multiple_of(b * 8, 8)
+            for h in range(heads):
+                values = v_s[pl.ds(base, 8), h * size : (h + 1) * size]
+                for j in range(8):
+                    line = values[j : j + 1, :]
+                    keep = tf[b, h, :, j : j + 1]
+                    new[l, base + j, h] = keep * (new[l, base + j, h] - line) + line
 
         def collect(s, carry):
             total, powers = carry

time: 63.1 us -> 52.3 us (0.83)
  Pallas kernels: 56.9 us -> 46.1 us
    pallas_call x1, Pallas kernels: 56.9 us -> 46.1 us  [body(): pl.pallas_call(functools.partial(kernel, n), out_shape=(jax.ShapeDtypeStr...]
where the time goes in v2:
time: 52.3 us; the launch traced here: 52.2 us
  Pallas kernels  46.1 us (88%)
  local copies, waits for them, and re-layouts  5.39 us (10%)
  between operations  0.65 us (1%)
    pallas_call x1, Pallas kernels, body(): pl.pallas_call(functools.partial(kernel, n), out_shape=(jax.ShapeDtypeStr...  46.1 us
    unnamed x4, local copies, waits for them, and re-layouts  5.39 us

profile of v2, /device:TPU:0, one launch (start us, length us, event | category | flops | bytes accessed | tf_op | source)
XLA Modules:
  0.0 52.2 jit_solution(6236378775637316944)
XLA Ops:
  0.6 46.1 %shard_map.113 = (bf16[48,256]{1,0:T(8,128)(2,1)}, f32[2,48,2,128,128]{4,3,2,1,0:T(8,128)S(1)}) custom-call(bf16[48,256]{1,0:T(8,128)(2,1)} %tok.1, f32[2,48,2,128,128]{4,3,2,1,0:T(8,128)} %states.1, f32[2,4096]{1,0:T(2,128)} %gain.1, bf16[2,4096,256]{2,1,0:T(8,128)(2,1)} %wq.1, bf16[2,4096,256]{2,1,0:T(8,128)(2,1)} %wf.1, bf16[2,4096,256]{2,1,0:T(8,128)(2,1)} %wv.1, ...), custom_call_target="tpu_custom_call" | custom-call | tf_op jit(solution)/shard_map/pallas_call | solution.py:351
  46.8 0.0 copy-start
  46.8 4.8 %copy.14 = f32[2,48,2,128,128]{4,3,2,1,0:T(8,128)} copy(f32[2,48,2,128,128]{4,3,2,1,0:T(8,128)S(1)} %get-tuple-element.3) | data formatting | bytes 25165824
  51.6 0.0 copy-done
  51.6 0.6 %copy.15 = bf16[48,256]{1,0:T(8,128)(2,1)} copy(bf16[48,256]{1,0:T(8,128)(2,1)S(1)} %copy-done) | data formatting | bytes 49152
Async XLA Ops:
  46.8 4.8 %copy-start = (bf16[48,256]{1,0:T(8,128)(2,1)S(1)}, bf16[48,256]{1,0:T(8,128)(2,1)}, u32[]{:S(2)}) copy-start(bf16[48,256]{1,0:T(8,128)(2,1)} %get-tuple-element.6) | copy-start | bytes 73732
